TPU v7x, 512 devices: a whole 4x8x8 slice. The times are simulated.
512 devices in a mesh: sp: 128 (over z, y, core), tp: 4 (over x).
Axes of the slice: x: 4, y: 8, z: 8, core: 2. Of those that a mesh axis runs over, the one named last changes fastest.
Arguments:
- tokens: bfloat16 [16384, 2048], P(('sp', 'tp')), may hold values from -6 to 6
- norm_gain: float32 [2048], replicated, may hold values from 0.1 to 1.9
- w_filter_b: bfloat16 [2048, 1024], P('sp', 'tp'), may hold values from -0.125 to 0.125
- w_filter_c: bfloat16 [2048, 1024], P('sp', 'tp'), may hold values from -0.125 to 0.125
- w_filter_v: bfloat16 [2048, 1024], P('sp', 'tp'), may hold values from -0.125 to 0.125
- filter_taps: float32 [3, 1024], P(None, 'tp'), may hold values from -3.5 to 3.5
- w_query: bfloat16 [2048, 1024], P('sp', 'tp'), may hold values from -0.125 to 0.125
- retention_gate_matrix: bfloat16 [2048, 1024], P('sp', 'tp'), may hold values from -0.125 to 0.125
- w_input: bfloat16 [2048, 1024], P('sp', 'tp'), may hold values from -0.125 to 0.125
- forget_gap: float32 [1024], P('tp'), may hold values from 0 to 0.12
- additive_fade_log: float32 [16384, 1024], P('sp', 'tp'), may hold values from -1.1 to 0
- head_gain: float32 [128], replicated, may hold values from 0.1 to 1.9
- initial_state: float32 [8, 128, 128], P('tp'), may hold values from -0.013671875 to 0.013671875
- w_out_filter: bfloat16 [1024, 2048], P('tp'), may hold values from -0.125 to 0.125
- w_out_rec: bfloat16 [1024, 2048], P('tp'), may hold values from -0.125 to 0.125
Outputs:
- mixed: bfloat16 [16384, 2048], P(('sp', 'tp'))
All inputs are finite; a program needn't handle non-finite values.
Results may differ from a plain program's by a relative error of at most 0.03.
Values may be sent and summed in bfloat16 or wider, within the bound.
No kernel may reach another device: no remote copies, remote signals or barrier semaphores. Data moves between devices by JAX's collectives and lax.ppermute only.
A program may use at most 64 MiB of HBM per device.

v0:
```python
import jax
import jax.numpy as jnp
import numpy as np
from jax import lax
from jax.sharding import Mesh
from jax.sharding import PartitionSpec as P

HEAD_DIM = 128
SPAN = 64
TAPS = 3
HALO = 16
SP = ("sp_0", "sp_1", "sp_2")
SP_TP = ("sp_0", "sp_1", "sp_2", "tp")
epsilon = 1e-06
f32 = jnp.float32
bf16 = jnp.bfloat16


def exchanged(blocks, axis):
    return lax.all_to_all(blocks, axis, split_axis=0, concat_axis=0, tiled=True)


def sent_to_all(x, axis):
    return exchanged(jnp.broadcast_to(x, (lax.axis_size(axis), *x.shape)), axis)


def swapped(x, axis):
    return lax.ppermute(x, axis, [(0, 1), (1, 0)])


def shifted(block, axis):
    size = lax.axis_size(axis)
    return lax.ppermute(block, axis, [(i, i + 1) for i in range(size - 1)])


def running_sum(x):
    causal = jnp.tril(jnp.ones((x.shape[0], x.shape[0]), f32))
    return jnp.dot(causal, x, precision=lax.Precision.HIGHEST)


def rates(forget_logit, forget_gap, fade):
    key_rate = forget_gap * jax.nn.sigmoid(-forget_logit.astype(f32))
    return (key_rate, jnp.log1p(-key_rate) + fade)


def silu(v):
    return jax.nn.silu(v.astype(f32))


def state_of(key_rate, log_decay, value_in):
    running = running_sum(log_decay)
    remainder = (key_rate * jnp.exp(running[-1:] - running)).astype(bf16)
    state = jnp.einsum("tv,tk->vk", value_in.astype(bf16), remainder, preferred_element_type=f32)
    return (running[-1], state)


def pack(decay, state):
    high = lax.reduce_precision(decay, 8, 7)
    rest = decay - high
    low = lax.reduce_precision(rest, 8, 7)
    rows = jnp.stack([high, low, rest - low]).astype(bf16)
    return jnp.concatenate([state.astype(bf16), rows, jnp.zeros((13, HEAD_DIM), bf16)], axis=0)


def unpack(packed):
    decays = packed[:, HEAD_DIM : HEAD_DIM + 3].astype(f32).sum(axis=1)
    return (decays, packed[:, :HEAD_DIM])


def weights_before(decays, position):
    size = decays.shape[0]
    place = jnp.arange(size)
    earlier = place < position
    kept = jnp.where(earlier[:, None], decays, 0.0)
    after = (place[None, :] > place[:, None]).astype(f32)
    since = jnp.sum(after[:, :, None] * kept[None], axis=1)
    return (jnp.where(earlier[:, None], jnp.exp(since), 0.0), kept.sum(axis=0))


def weighted(weights, states):
    return jnp.sum(weights[:, None, :] * states.astype(f32), axis=0)


def body(
    tokens,
    norm_gain,
    w_filter_b,
    w_filter_c,
    w_filter_v,
    filter_taps,
    w_query,
    retention_gate_matrix,
    w_input,
    forget_gap,
    additive_fade_log,
    head_gain,
    initial_state,
    w_out_filter,
    w_out_rec,
):
    z, y, c = (lax.axis_index(a) for a in SP)
    own_rows = jnp.concatenate(
        [retention_gate_matrix, w_input, w_query, w_filter_b, w_filter_c, w_filter_v], axis=1
    )
    along_y = sent_to_all(own_rows, "sp_1").reshape(-1, own_rows.shape[1])
    weights = lax.all_gather(along_y, ("sp_0", "sp_2"), axis=0, tiled=True)
    gathered = sent_to_all(tokens, "tp").reshape(-1, tokens.shape[1])
    widened = gathered.astype(f32)
    normed = (
        widened
        * lax.rsqrt(jnp.mean(widened * widened, axis=-1, keepdims=True) + epsilon)
        * norm_gain
    ).astype(bf16)
    length, width = normed.shape
    order = np.arange(256).reshape(8, 2, 16).transpose(1, 0, 2).reshape(-1)
    swap = np.zeros((256, 256), np.float32)
    swap[order, np.arange(256)] = 1.0
    own = (
        jnp.einsum(
            "tzk,kl->tzl",
            normed.reshape(length, 8, 256),
            jnp.asarray(swap, bf16),
            preferred_element_type=f32,
        )
        .astype(bf16)
        .reshape(length, width)
    )
    partner = swapped(own, "sp_2")
    halo = shifted(own[length - HALO :], SP)
    fade = additive_fade_log
    head = lambda a, k: lax.dynamic_slice_in_dim(a, k * HEAD_DIM, HEAD_DIM, axis=1)
    partner_fade = swapped(head(fade, 1 - c), "sp_2")
    chip = jnp.concatenate([own, partner], axis=0)
    chip_gates = jnp.dot(chip, weights[:, :512], preferred_element_type=f32).astype(bf16)
    forget_logit, input_value = (chip_gates[:, :256], chip_gates[:, 256:])
    key_rate, log_decay = rates(forget_logit[:length], forget_gap, fade)
    value_in = silu(input_value[:length])
    gap_c = lax.dynamic_slice_in_dim(forget_gap, c * HEAD_DIM, HEAD_DIM)
    partner_rate, partner_decay = rates(head(forget_logit[length:], c), gap_c, partner_fade)
    partner_value = silu(head(input_value[length:], c))
    decay_own, state_own = state_of(head(key_rate, c), head(log_decay, c), head(value_in, c))
    decay_partner, state_partner = state_of(partner_rate, partner_decay, partner_value)
    first = c == 0
    decay_0, decay_1 = (
        jnp.where(first, decay_own, decay_partner),
        jnp.where(first, decay_partner, decay_own),
    )
    state_0, state_1 = (
        jnp.where(first, state_own, state_partner),
        jnp.where(first, state_partner, state_own),
    )
    state_chip = jnp.exp(decay_1)[None, :] * state_0 + state_1
    decays_y, states_y = unpack(sent_to_all(pack(decay_0 + decay_1, state_chip), "sp_1"))
    weights_row, decay_row = weights_before(decays_y, 8)
    row = weighted(weights_row, states_y)
    decays_z, states_z = unpack(sent_to_all(pack(decay_row, row), "sp_0"))
    weights_y, decay_y = weights_before(decays_y, y)
    inside = weighted(weights_y, states_y)
    weights_z, decay_z = weights_before(decays_z, z)
    start = lax.dynamic_index_in_dim(initial_state, c, keepdims=False).T
    before = jnp.exp(decay_z)[None, :] * start + weighted(weights_z, states_z)
    into_chip = jnp.exp(decay_y)[None, :] * before + inside
    into_second = jnp.exp(decay_0)[None, :] * into_chip + state_0
    incoming = exchanged(jnp.stack([into_chip, into_second]).astype(bf16), "sp_2")
    rest = jnp.dot(
        jnp.concatenate([halo, own], axis=0), weights[:, 512:], preferred_element_type=f32
    ).astype(bf16)
    queries = rest[HALO:, :256].astype(f32)
    gate_out = rest[HALO:, 256:512].astype(f32)
    product = rest[:, 512:768].astype(f32) * rest[:, 768:].astype(f32)
    filtered = jnp.zeros_like(gate_out)
    for offset in range(TAPS):
        at = HALO - (TAPS - 1) + offset
        filtered = filtered + filter_taps[offset] * product[at : at + length]
    filter_out = (gate_out * filtered).astype(bf16)
    filter_part = jnp.dot(filter_out, w_out_filter, preferred_element_type=f32)
    heads = lambda a: a.reshape(length // SPAN, SPAN, 2, HEAD_DIM)
    running = running_sum(log_decay)
    at_start = jnp.concatenate([jnp.zeros((1, 256), f32), running[SPAN - 1 : length - 1 : SPAN]])
    at_end = running[SPAN - 1 :: SPAN]
    within = running.reshape(length // SPAN, SPAN, 256) - at_start[:, None]
    scaled_query = heads((queries.reshape(within.shape) * jnp.exp(within)).astype(bf16))
    scaled_key = heads((key_rate.reshape(within.shape) * jnp.exp(-within)).astype(bf16))
    remainder = heads(
        (
            key_rate.reshape(within.shape)
            * jnp.exp(at_end[:, None] - running.reshape(within.shape))
        ).astype(bf16)
    )
    values = heads(value_in.astype(bf16))
    causal = jnp.tril(jnp.ones((SPAN, SPAN), dtype=bool))
    scores = jnp.einsum("bthk,bshk->bhts", scaled_query, scaled_key, preferred_element_type=f32)
    scores = jnp.where(causal, scores, 0.0).astype(bf16)
    local = jnp.einsum("bhts,bshv->bthv", scores, values, preferred_element_type=f32)
    cross = jnp.einsum("thk,shk->hts", scaled_query[1], remainder[0], preferred_element_type=f32)
    cross = jnp.einsum("hts,shv->thv", cross.astype(bf16), values[0], preferred_element_type=f32)
    local = jnp.concatenate([local[0], local[1] + cross], axis=0)
    full_query = (queries * jnp.exp(running)).astype(bf16).reshape(length, 2, HEAD_DIM)
    raw = local + jnp.einsum("thk,hvk->thv", full_query, incoming, preferred_element_type=f32)
    rec_out = (
        (raw * lax.rsqrt(jnp.mean(raw * raw, axis=-1, keepdims=True) + epsilon) * head_gain)
        .astype(bf16)
        .reshape(length, -1)
    )
    partial = (filter_part + jnp.dot(rec_out, w_out_rec, preferred_element_type=f32)).astype(bf16)
    arrived = exchanged(partial.reshape(4, length // 4, -1), "tp")
    return arrived.astype(f32).sum(axis=0).astype(bf16)


def solution(mesh):
    torus = Mesh(mesh.devices.reshape(8, 8, 2, mesh.shape["tp"]), ("sp_0", "sp_1", "sp_2", "tp"))
    placed = (
        P(SP_TP, None),
        P(),
        P(SP, "tp"),
        P(SP, "tp"),
        P(SP, "tp"),
        P(None, "tp"),
        P(SP, "tp"),
        P(SP, "tp"),
        P(SP, "tp"),
        P("tp"),
        P(SP, "tp"),
        P(),
        P("tp", None, None),
        P("tp", None),
        P("tp", None),
    )
    return jax.shard_map(
        body, mesh=torus, in_specs=placed, out_specs=P(SP_TP, None), check_vma=False
    )
```

profile of v0, /device:TPU:1, one launch (start us, length us, event | category | flops | bytes accessed | tf_op | source)
XLA Modules:
  0.0 157.7 jit_solution(3976584171746836471)
XLA Ops:
  6.6 0.8 constant_dynamic-update-slice_fusion.5
  7.4 0.7 constant_dynamic-update-slice_fusion.4
  8.1 0.7 constant_dynamic-update-slice_fusion.3
  8.8 0.7 constant_dynamic-update-slice_fusion.2
  9.5 0.7 constant_dynamic-update-slice_fusion.1
  10.2 0.7 constant_dynamic-update-slice_fusion
  10.9 19.2 %all_to_all.30 = bf16[8,16,1536]{2,1,0:T(8,128)(2,1)} all-to-all(bf16[8,16,1536]{2,1,0:T(8,128)(2,1)S(1)} %broadcast_in_dim.102), channel_id=1, replica_groups=mesh['sp_0'=8,'sp_1'=8,'sp_2'=2,'tp'=4] {'sp_1'}, dimensions={0} | all-to-all | bytes 786432 | tf_op jit(solution)/shard_map/all_to_all | solution.py:20
  30.1 1.8 %broadcast_in_dim.101 = bf16[4,32,2048]{2,1,0:T(8,128)(2,1)} broadcast(bf16[32,2048]{1,0:T(8,128)(2,1)} %param.16), dimensions={1,2} | broadcast | bytes 655360 | tf_op jit(solution)/shard_map/broadcast_in_dim | solution.py:24
  31.9 6.0 %all-to-all-start = ((bf16[4,32,2048]{2,1,0:T(8,128)(2,1)}), bf16[4,32,2048]{2,1,0:T(8,128)(2,1)S(1)}, u32[]{:S(2)}, u32[]{:S(2)}) async-start(bf16[4,32,2048]{2,1,0:T(8,128)(2,1)} %broadcast_in_dim.101), calls=%async_computation | async-start | bytes 1048576 | tf_op jit(solution)/shard_map/all_to_all | solution.py:20
  37.8 4.4 %collective-permute-start.2 = (f32[128,128]{1,0:T(8,128)S(1)}, f32[128,128]{1,0:T(8,128)S(1)}, u32[]{:S(2)}, u32[]{:S(2)}) collective-permute-start(f32[128,128]{1,0:T(8,128)S(1)} %constant_dynamic-slice_fusion.1), channel_id=1, source_target_pairs={{0,4},{4,0},{1,5},{5,1},{2,6},{6,2},{3,7},{7,3},{8,12},{12,8},{9,1... | collective-permute-start | bytes 196616 | tf_op jit(solution)/shard_map/ppermute | solution.py:28
  42.3 0.1 copy.95
  42.4 0.1 dynamic_slice.25
  42.5 2.3 %all-to-all-done = bf16[4,32,2048]{2,1,0:T(8,128)(2,1)S(1)} async-done(((bf16[4,32,2048]{2,1,0:T(8,128)(2,1)}), bf16[4,32,2048]{2,1,0:T(8,128)(2,1)S(1)}, u32[]{:S(2)}, u32[]{:S(2)}) %all-to-all-start) | async-done | bytes 524320 | tf_op jit(solution)/shard_map/all_to_all | solution.py:20
  44.8 0.1 copy.105
  44.9 0.2 multiply_reduce_fusion
  45.1 0.1 rsqrt.20
  45.2 0.2 fusion.15
  45.4 0.3 convolution_convert_fusion
  45.8 0.3 copy.84
  46.0 5.4 %collective-permute-start.1 = (bf16[128,2048]{0,1:T(8,128)(2,1)S(1)}, bf16[128,2048]{0,1:T(8,128)(2,1)}, u32[]{:S(2)}, u32[]{:S(2)}) collective-permute-start(bf16[128,2048]{0,1:T(8,128)(2,1)S(1)} %bitcast.98), channel_id=1, source_target_pairs={{0,4},{4,0},{1,5},{5,1},{2,6},{6,2},{3,7},{7,3},{8,12},{12,8},{9,1... | collective-permute-start | bytes 1572872 | tf_op jit(solution)/shard_map/ppermute | solution.py:28
  51.5 2.2 %collective-permute-start = (bf16[16,2048]{1,0:T(8,128)(2,1)S(1)}, bf16[16,2048]{1,0:T(8,128)(2,1)S(1)}, u32[]{:S(2)}, u32[]{:S(2)}) collective-permute-start(bf16[16,2048]{1,0:T(8,128)(2,1)S(1)} %bitcast.102), channel_id=1, source_target_pairs={{0,4},{4,8},{8,12},{12,16},{16,20},{20,24},{24,28},{28,32},{32,36}... | collective-permute-start | bytes 196616 | tf_op jit(solution)/shard_map/ppermute | solution.py:33
  53.6 1.3 collective-permute-done
  54.9 0.3 copy.85
  55.2 28.0 %all-gather.2.cloned.1.call-done = bf16[2048,1536]{1,0:T(8,128)(2,1)} async-done(((bf16[128,1536]{1,0:T(8,128)(2,1)}), bf16[2048,1536]{1,0:T(8,128)(2,1)}) %all-gather.2.cloned.1.call-update) | async-done | bytes 6291472 | tf_op jit(solution)/shard_map/all_gather | solution.py:106
  83.3 2.6 %fusion.8 = bf16[256,512]{1,0:T(8,128)(2,1)S(1)} fusion(bf16[2048,1536]{1,0:T(8,128)(2,1)} %all-gather.2.cloned.1.call-done, bf16[128,2048]{0,1:T(8,128)(2,1)} %collective-permute-done.1, bf16[128,2048]{0,1:T(8,128)(2,1)S(1)} %bitcast.99), kind=kOutput, calls=%fused_computation.8 | convolution fusion | flops 539099136 | bytes 3407872 | tf_op jit(solution)/shard_map/dot_general | solution.py:134
  85.9 0.1 divide_multiply_fusion
  86.1 0.8 copy-done.9
  86.9 1.3 fusion.5
  88.2 0.3 fusion.38
  88.5 0.2 fusion.34
  88.7 0.3 fusion.36
  89.0 0.6 exponential_bitcast_fusion
  89.6 0.2 fusion.74
  89.8 0.8 add_convert_fusion.1
  90.6 0.2 concatenate.28
  90.8 0.7 broadcast_in_dim.107
  91.5 6.0 %all-to-all-start.2 = ((bf16[8,144,128]{2,1,0:T(8,128)(2,1)}), bf16[8,144,128]{2,1,0:T(8,128)(2,1)S(1)}, u32[]{:S(2)}, u32[]{:S(2)}) async-start(bf16[8,144,128]{2,1,0:T(8,128)(2,1)} %broadcast_in_dim.107), calls=%async_computation.2 | async-start | bytes 589824 | tf_op jit(solution)/shard_map/all_to_all | solution.py:20
  97.5 0.1 reshape.247
  97.6 0.1 reshape.248
  97.8 0.1 reshape.246
  97.9 0.3 convolution_bitcast_fusion
  98.2 12.3 %all-to-all-done.2 = bf16[8,144,128]{2,1,0:T(8,128)(2,1)S(1)} async-done(((bf16[8,144,128]{2,1,0:T(8,128)(2,1)}), bf16[8,144,128]{2,1,0:T(8,128)(2,1)S(1)}, u32[]{:S(2)}, u32[]{:S(2)}) %all-to-all-start.2) | async-done | bytes 294944 | tf_op jit(solution)/shard_map/all_to_all | solution.py:20
  110.4 0.1 fusion.111
  110.5 0.1 multiply_reduce_fusion.5
  110.8 0.7 fusion.22
  111.5 0.2 concatenate.29
  111.6 0.7 broadcast_in_dim.111
  112.4 3.9 %all-to-all-start.3 = ((bf16[8,144,128]{2,1,0:T(8,128)(2,1)}), bf16[8,144,128]{2,1,0:T(8,128)(2,1)S(1)}, u32[]{:S(2)}, u32[]{:S(2)}) async-start(bf16[8,144,128]{2,1,0:T(8,128)(2,1)} %broadcast_in_dim.111), calls=%async_computation.3 | async-start | bytes 589824 | tf_op jit(solution)/shard_map/all_to_all | solution.py:20
  116.3 0.6 slice_bitcast_fusion.1
  116.9 0.9 fusion.13
  117.8 0.3 fusion.49
  118.1 9.4 %all-to-all-done.3 = bf16[8,144,128]{2,1,0:T(8,128)(2,1)S(1)} async-done(((bf16[8,144,128]{2,1,0:T(8,128)(2,1)}), bf16[8,144,128]{2,1,0:T(8,128)(2,1)S(1)}, u32[]{:S(2)}, u32[]{:S(2)}) %all-to-all-start.3) | async-done | bytes 294944 | tf_op jit(solution)/shard_map/all_to_all | solution.py:20
  127.6 0.1 fusion.112
  127.7 0.1 multiply_reduce_fusion.4
  127.8 0.1 exponential_select_fusion.1
  127.9 0.9 convert_bitcast_fusion
  128.9 0.9 fusion.75
  129.8 5.5 %all_to_all.31 = bf16[2,128,128]{2,1,0:T(8,128)(2,1)S(1)} all-to-all(bf16[2,128,128]{2,1,0:T(8,128)(2,1)S(1)} %pad_maximum_fusion), channel_id=1, replica_groups=mesh['sp_0'=8,'sp_1'=8,'sp_2'=2,'tp'=4] {'sp_2'}, dimensions={0} | all-to-all | bytes 131072 | tf_op jit(solution)/shard_map/all_to_all | solution.py:20
  135.2 1.2 multiply_reduce_fusion.2
  136.4 0.8 multiply_convert_fusion
  137.2 0.1 copy.98
  137.3 0.3 fusion.2
  137.7 12.4 %all_to_all.32 = bf16[4,32,2048]{2,1,0:T(8,128)(2,1)S(1)} all-to-all(bf16[4,32,2048]{2,1,0:T(8,128)(2,1)S(1)} %bitcast.94), channel_id=1, replica_groups=mesh['sp_0'=8,'sp_1'=8,'sp_2'=2,'tp'=4] {'tp'}, dimensions={0} | all-to-all | bytes 1048576 | tf_op jit(solution)/shard_map/all_to_all | solution.py:20
  150.1 0.7 reduce_sum.145
  (63 shorter events, 0.7 us)
Async XLA Ops:
  6.5 111.3 %copy-start = (bf16[256,2048]{1,0:T(8,128)(2,1)S(1)}, bf16[256,2048]{1,0:T(8,128)(2,1)}, u32[]{:S(2)}) copy-start(bf16[256,2048]{1,0:T(8,128)(2,1)} %param.29) | copy-start | bytes 3145732
  6.5 31.3 %copy-start.3 = (f32[128,256]{1,0:T(8,128)S(1)}, f32[128,256]{1,0:T(8,128)}, u32[]{:S(2)}) copy-start(f32[128,256]{1,0:T(8,128)} %param.26) | copy-start | bytes 393220
  6.5 35.7 %copy-start.5 = (f32[2,128,128]{2,1,0:T(8,128)S(1)}, f32[2,128,128]{2,1,0:T(8,128)}, u32[]{:S(2)}) copy-start(f32[2,128,128]{2,1,0:T(8,128)} %param.28) | copy-start | bytes 393220
  6.5 35.7 %copy-start.6 = (f32[2048]{0:T(1024)S(1)}, f32[2048]{0:T(1024)}, u32[]{:S(2)}) copy-start(f32[2048]{0:T(1024)} %param.17) | copy-start | bytes 24580
  6.5 35.9 %copy-start.8 = (f32[256]{0:T(256)S(1)}, f32[256]{0:T(256)}, u32[]{:S(2)}) copy-start(f32[256]{0:T(256)} %param.25) | copy-start | bytes 3076
  6.5 76.7 %all-gather.2.cloned.1.call-start = ((), (), s32[]{:S(2)}) async-start(), calls=%async_computation.6 | async-start | bytes 6684672 | tf_op jit(solution)/shard_map/all_gather | solution.py:106
  31.9 12.9 %all-to-all-start = ((bf16[4,32,2048]{2,1,0:T(8,128)(2,1)}), bf16[4,32,2048]{2,1,0:T(8,128)(2,1)S(1)}, u32[]{:S(2)}, u32[]{:S(2)}) async-start(bf16[4,32,2048]{2,1,0:T(8,128)(2,1)} %broadcast_in_dim.101), calls=%async_computation | async-start | bytes 1048576 | tf_op jit(solution)/shard_map/all_to_all | solution.py:20
  37.8 7.6 %copy-start.4 = (bf16[256,256,1]{1,0,2:T(8,128)(2,1)S(1)}, bf16[256,256,1]{1,0,2:T(8,128)(2,1)}, u32[]{:S(2)}) copy-start(bf16[256,256,1]{1,0,2:T(8,128)(2,1)} %constant.72) | copy-start | bytes 393220
  37.8 50.8 %collective-permute-start.2 = (f32[128,128]{1,0:T(8,128)S(1)}, f32[128,128]{1,0:T(8,128)S(1)}, u32[]{:S(2)}, u32[]{:S(2)}) collective-permute-start(f32[128,128]{1,0:T(8,128)S(1)} %constant_dynamic-slice_fusion.1), channel_id=1, source_target_pairs={{0,4},{4,0},{1,5},{5,1},{2,6},{6,2},{3,7},{7,3},{8,12},{12,8},{9,1... | collective-permute-start | bytes 196616 | tf_op jit(solution)/shard_map/ppermute | solution.py:28
  44.9 6.5 %copy-start.7 = (f32[3,256]{1,0:T(4,128)S(1)}, f32[3,256]{1,0:T(4,128)}, u32[]{:S(2)}) copy-start(f32[3,256]{1,0:T(4,128)} %param.21) | copy-start | bytes 9220
  46.0 9.2 %collective-permute-start.1 = (bf16[128,2048]{0,1:T(8,128)(2,1)S(1)}, bf16[128,2048]{0,1:T(8,128)(2,1)}, u32[]{:S(2)}, u32[]{:S(2)}) collective-permute-start(bf16[128,2048]{0,1:T(8,128)(2,1)S(1)} %bitcast.98), channel_id=1, source_target_pairs={{0,4},{4,0},{1,5},{5,1},{2,6},{6,2},{3,7},{7,3},{8,12},{12,8},{9,1... | collective-permute-start | bytes 1572872 | tf_op jit(solution)/shard_map/ppermute | solution.py:28
  51.5 3.5 %collective-permute-start = (bf16[16,2048]{1,0:T(8,128)(2,1)S(1)}, bf16[16,2048]{1,0:T(8,128)(2,1)S(1)}, u32[]{:S(2)}, u32[]{:S(2)}) collective-permute-start(bf16[16,2048]{1,0:T(8,128)(2,1)S(1)} %bitcast.102), channel_id=1, source_target_pairs={{0,4},{4,8},{8,12},{12,16},{16,20},{20,24},{24,28},{28,32},{32,36}... | collective-permute-start | bytes 196616 | tf_op jit(solution)/shard_map/ppermute | solution.py:33
  83.3 3.6 %copy-start.9 = (bf16[2048,1536]{1,0:T(8,128)(2,1)S(1)}, bf16[2048,1536]{1,0:T(8,128)(2,1)}, u32[]{:S(2)}) copy-start(bf16[2048,1536]{1,0:T(8,128)(2,1)} %all-gather.2.cloned.1.call-done) | copy-start | bytes 18874372
  88.1 29.7 %copy-start.2 = (bf16[144,1024]{1,0:T(8,128)(2,1)}, bf16[144,1024]{1,0:T(8,128)(2,1)S(1)}, u32[]{:S(2)}) copy-start(bf16[144,1024]{1,0:T(8,128)(2,1)S(1)} %fusion.5) | copy-start | bytes 884740
  91.5 18.9 %all-to-all-start.2 = ((bf16[8,144,128]{2,1,0:T(8,128)(2,1)}), bf16[8,144,128]{2,1,0:T(8,128)(2,1)S(1)}, u32[]{:S(2)}, u32[]{:S(2)}) async-start(bf16[8,144,128]{2,1,0:T(8,128)(2,1)} %broadcast_in_dim.107), calls=%async_computation.2 | async-start | bytes 589824 | tf_op jit(solution)/shard_map/all_to_all | solution.py:20
  112.4 15.2 %all-to-all-start.3 = ((bf16[8,144,128]{2,1,0:T(8,128)(2,1)}), bf16[8,144,128]{2,1,0:T(8,128)(2,1)S(1)}, u32[]{:S(2)}, u32[]{:S(2)}) async-start(bf16[8,144,128]{2,1,0:T(8,128)(2,1)} %broadcast_in_dim.111), calls=%async_computation.3 | async-start | bytes 589824 | tf_op jit(solution)/shard_map/all_to_all | solution.py:20
  127.9 9.4 %copy-start.1 = (bf16[256,2048]{1,0:T(8,128)(2,1)S(1)}, bf16[256,2048]{1,0:T(8,128)(2,1)}, u32[]{:S(2)}) copy-start(bf16[256,2048]{1,0:T(8,128)(2,1)} %param.30) | copy-start | bytes 3145732
Sparse Core Ops, SparseCore 0:
  30.2 53.0 all-gather.1
where the time goes:
time: 159 us; the launch traced here: 158 us
  waiting for transfers between devices  53.3 us (34%)
  blocking collectives  37 us (23%)
  starting transfers between devices  27.8 us (17%)
  between operations  13.9 us (9%)
  local copies, waits for them, and re-layouts  10.7 us (7%)
  matrix products  8.98 us (6%)
  other arithmetic  5.94 us (4%)
    all_to_all x3, blocking collectives, exchanged(): return lax.all_to_all(blocks, axis, split_axis=0, concat_axis=0, tiled=True)  37 us
    all_gather x1, waiting for transfers between devices, body(): weights = lax.all_gather(along_y, ('sp_0', 'sp_2'), axis=0, tiled=True)  28 us
    all_to_all x3, waiting for transfers between devices, exchanged(): return lax.all_to_all(blocks, axis, split_axis=0, concat_axis=0, tiled=True)  24 us
    all_to_all x3, starting transfers between devices, exchanged(): return lax.all_to_all(blocks, axis, split_axis=0, concat_axis=0, tiled=True)  15.8 us
    ppermute x2, starting transfers between devices, swapped(): return lax.ppermute(x, axis, [(0, 1), (1, 0)])  9.76 us
    unnamed x27, local copies, waits for them, and re-layouts  4.51 us
    broadcast_in_dim x4, local copies, waits for them, and re-layouts, sent_to_all(): return exchanged(jnp.broadcast_to(x, (lax.axis_size(axis), *x.shape)), axis)  3.29 us
  transfers between devices with their start and end apart: 7, of which 5 were waited for; matrix products, arithmetic and copies ran while one was open for 7% of the time, Pallas kernels for 0%

commit v1 on v0

--- a/solution.py
+++ b/solution.py
@@ -103,7 +103,12 @@
         [retention_gate_matrix, w_input, w_query, w_filter_b, w_filter_c, w_filter_v], axis=1
     )
     along_y = sent_to_all(own_rows, "sp_1").reshape(-1, own_rows.shape[1])
-    weights = lax.all_gather(along_y, ("sp_0", "sp_2"), axis=0, tiled=True)
+    weights = jnp.concatenate(
+        lax.all_to_all(
+            jnp.stack([along_y] * lax.axis_size(("sp_0", "sp_2"))), ("sp_0", "sp_2"), 0, 0
+        ),
+        axis=0,
+    )
     gathered = sent_to_all(tokens, "tp").reshape(-1, tokens.shape[1])
     widened = gathered.astype(f32)
     normed = (

time: 159 us -> 254 us (1.60)
  waiting for transfers between devices: 53.3 us -> 154 us
  between operations: 13.9 us -> 0.55 us
  starting transfers between devices: 27.8 us -> 36.8 us
  other arithmetic: 5.94 us -> 2.32 us
    all_to_all x0 -> x1, waiting for transfers between devices: none -> 128 us  [body(): lax.all_to_all(jnp.stack([along_y] * lax.axis_size(('sp_0', 'sp_2'))), ('...]
    all_gather x1 -> x0, waiting for transfers between devices: 28 us -> none  [body(): weights = lax.all_gather(along_y, ('sp_0', 'sp_2'), axis=0, tiled=True)]
    all_to_all x0 -> x1, starting transfers between devices: none -> 14.5 us  [body(): lax.all_to_all(jnp.stack([along_y] * lax.axis_size(('sp_0', 'sp_2'))), ('...]
    ppermute x2, starting transfers between devices: 9.76 us -> 4.46 us  [swapped(): return lax.ppermute(x, axis, [(0, 1), (1, 0)])]
    another operation x1 -> x2, local copies, waits for them, and re-layouts: 0.01 us -> 3.27 us  [the longest x1 3.26 us: body(): jnp.stack([along_y] * lax.axis_size(('sp_0', 'sp_2')))]
  transfers between devices with their start and end apart: 7 -> 7, of which waited for: 5 -> 5; matrix products, arithmetic and copies ran while one was open for 7% -> 5% of each run, Pallas kernels for 0% -> 0%
where the time goes in v1:
time: 254 us; the launch traced here: 253 us
  waiting for transfers between devices  154 us (61%)
  starting transfers between devices  36.8 us (14%)
  blocking collectives  36.5 us (14%)
  local copies, waits for them, and re-layouts  12.6 us (5%)
  matrix products  10.1 us (4%)
    all_to_all x1, waiting for transfers between devices, body(): lax.all_to_all(jnp.stack([along_y] * lax.axis_size(('sp_0', 'sp_2'))), ('...  128 us
    all_to_all x3, blocking collectives, exchanged(): return lax.all_to_all(blocks, axis, split_axis=0, concat_axis=0, tiled=True)  36.5 us
    all_to_all x3, waiting for transfers between devices, exchanged(): return lax.all_to_all(blocks, axis, split_axis=0, concat_axis=0, tiled=True)  24.4 us
    all_to_all x3, starting transfers between devices, exchanged(): return lax.all_to_all(blocks, axis, split_axis=0, concat_axis=0, tiled=True)  15.6 us
    all_to_all x1, starting transfers between devices, body(): lax.all_to_all(jnp.stack([along_y] * lax.axis_size(('sp_0', 'sp_2'))), ('...  14.5 us
  transfers between devices with their start and end apart: 7, of which 5 were waited for; matrix products, arithmetic and copies ran while one was open for 5% of the time, Pallas kernels for 0%

profile of v1, /device:TPU:1, one launch (start us, length us, event | category | flops | bytes accessed | tf_op | source)
XLA Modules:
  0.0 252.9 jit_solution(19449111124146691)
XLA Ops:
  0.0 1.8 broadcast_in_dim.101
  1.8 4.8 %all-to-all-start = ((bf16[4,32,2048]{2,1,0:T(8,128)(2,1)}), bf16[4,32,2048]{2,1,0:T(8,128)(2,1)S(1)}, u32[]{:S(2)}, u32[]{:S(2)}) async-start(bf16[4,32,2048]{2,1,0:T(8,128)(2,1)} %broadcast_in_dim.101), calls=%async_computation | async-start | bytes 1048576 | tf_op jit(solution)/shard_map/all_to_all | solution.py:20
  6.7 0.7 constant_dynamic-update-slice_fusion.5
  7.4 0.7 constant_dynamic-update-slice_fusion.4
  8.1 0.7 constant_dynamic-update-slice_fusion.3
  8.8 0.7 constant_dynamic-update-slice_fusion.2
  9.5 0.7 constant_dynamic-update-slice_fusion.1
  10.2 0.7 constant_dynamic-update-slice_fusion
  10.9 2.7 %all-to-all-done = bf16[4,32,2048]{2,1,0:T(8,128)(2,1)S(1)} async-done(((bf16[4,32,2048]{2,1,0:T(8,128)(2,1)}), bf16[4,32,2048]{2,1,0:T(8,128)(2,1)S(1)}, u32[]{:S(2)}, u32[]{:S(2)}) %all-to-all-start) | async-done | bytes 524320 | tf_op jit(solution)/shard_map/all_to_all | solution.py:20
  13.6 19.6 %all_to_all.35 = bf16[8,16,1536]{2,1,0:T(8,128)(2,1)S(1)} all-to-all(bf16[8,16,1536]{2,1,0:T(8,128)(2,1)S(1)} %broadcast_in_dim.102), channel_id=1, replica_groups=mesh['sp_0'=8,'sp_1'=8,'sp_2'=2,'tp'=4] {'sp_1'}, dimensions={0} | all-to-all | bytes 786432 | tf_op jit(solution)/shard_map/all_to_all | solution.py:20
  33.2 3.3 %stack.25 = bf16[16,128,1536]{2,1,0:T(8,128)(2,1)} broadcast(bf16[128,1536]{1,0:T(8,128)(2,1)S(1)} %bitcast.96), dimensions={1,2} | broadcast | bytes 6684672 | tf_op jit(solution)/shard_map/stack | solution.py:108
  36.5 14.5 %all-to-all-start.2 = ((bf16[16,128,1536]{2,1,0:T(8,128)(2,1)}), bf16[16,128,1536]{2,1,0:T(8,128)(2,1)}, u32[]{:S(2)}, u32[]{:S(2)}) async-start(bf16[16,128,1536]{2,1,0:T(8,128)(2,1)} %stack.25), calls=%async_computation.2 | async-start | bytes 12582912 | tf_op jit(solution)/shard_map/all_to_all | solution.py:107
  51.1 2.2 collective-permute-start.2
  53.4 0.1 copy.95
  53.5 0.1 dynamic_slice.25
  53.6 0.1 copy.105
  53.7 0.2 multiply_reduce_fusion
  53.9 0.1 rsqrt.20
  54.0 0.2 fusion.15
  54.2 0.3 convolution_convert_fusion
  54.5 0.3 copy.84
  54.8 2.3 collective-permute-start.1
  57.1 2.2 collective-permute-start
  59.4 1.3 collective-permute-done
  60.7 0.3 copy.85
  61.0 128.4 %all-to-all-done.2 = bf16[16,128,1536]{2,1,0:T(8,128)(2,1)} async-done(((bf16[16,128,1536]{2,1,0:T(8,128)(2,1)}), bf16[16,128,1536]{2,1,0:T(8,128)(2,1)}, u32[]{:S(2)}, u32[]{:S(2)}) %all-to-all-start.2) | async-done | bytes 6291488 | tf_op jit(solution)/shard_map/all_to_all | solution.py:107
  189.4 2.5 fusion.8
  191.9 0.1 divide_multiply_fusion
  192.1 3.5 %fusion.5 = bf16[144,1024]{1,0:T(8,128)(2,1)S(1)} fusion(bf16[2048,1536]{1,0:T(8,128)(2,1)} %bitcast.3, bf16[128,2048]{0,1:T(8,128)(2,1)S(1)} %bitcast.101, bf16[16,2048]{0,1:T(8,128)(2,1)S(1)} %copy.85), kind=kOutput, calls=%fused_computation.7 | convolution fusion | flops 605306880 | bytes 5079040 | tf_op jit(solution)/shard_map/dot_general | solution.py:170
  195.6 0.3 fusion.38
  195.9 0.2 fusion.34
  196.1 0.3 fusion.36
  196.4 0.2 fusion.74
  196.6 0.2 add_convert_fusion.1
  196.8 0.2 concatenate.28
  197.0 0.7 broadcast_in_dim.107
  197.8 3.6 %all-to-all-start.3 = ((bf16[8,144,128]{2,1,0:T(8,128)(2,1)}), bf16[8,144,128]{2,1,0:T(8,128)(2,1)S(1)}, u32[]{:S(2)}, u32[]{:S(2)}) async-start(bf16[8,144,128]{2,1,0:T(8,128)(2,1)} %broadcast_in_dim.107), calls=%async_computation.3 | async-start | bytes 589824 | tf_op jit(solution)/shard_map/all_to_all | solution.py:20
  201.3 0.1 reshape.249
  201.4 0.1 reshape.250
  201.5 0.1 reshape.248
  201.7 0.3 convolution_bitcast_fusion
  202.0 10.5 %all-to-all-done.3 = bf16[8,144,128]{2,1,0:T(8,128)(2,1)S(1)} async-done(((bf16[8,144,128]{2,1,0:T(8,128)(2,1)}), bf16[8,144,128]{2,1,0:T(8,128)(2,1)S(1)}, u32[]{:S(2)}, u32[]{:S(2)}) %all-to-all-start.3) | async-done | bytes 294944 | tf_op jit(solution)/shard_map/all_to_all | solution.py:20
  212.5 0.1 fusion.111
  212.6 0.1 multiply_reduce_fusion.5
  212.7 0.1 exponential_select_fusion.2
  212.8 0.1 exponential_select_fusion
  212.8 0.1 fusion.22
  212.9 0.2 concatenate.29
  213.1 0.7 broadcast_in_dim.111
  213.8 7.3 %all-to-all-start.4 = ((bf16[8,144,128]{2,1,0:T(8,128)(2,1)}), bf16[8,144,128]{2,1,0:T(8,128)(2,1)S(1)}, u32[]{:S(2)}, u32[]{:S(2)}) async-start(bf16[8,144,128]{2,1,0:T(8,128)(2,1)} %broadcast_in_dim.111), calls=%async_computation.4 | async-start | bytes 589824 | tf_op jit(solution)/shard_map/all_to_all | solution.py:20
  221.1 0.2 fusion.13
  221.4 0.3 fusion.49
  221.7 11.1 %all-to-all-done.4 = bf16[8,144,128]{2,1,0:T(8,128)(2,1)S(1)} async-done(((bf16[8,144,128]{2,1,0:T(8,128)(2,1)}), bf16[8,144,128]{2,1,0:T(8,128)(2,1)S(1)}, u32[]{:S(2)}, u32[]{:S(2)}) %all-to-all-start.4) | async-done | bytes 294944 | tf_op jit(solution)/shard_map/all_to_all | solution.py:20
  232.9 0.1 fusion.112
  233.0 0.1 multiply_reduce_fusion.4
  233.1 0.1 exponential_select_fusion.1
  233.1 0.1 multiply_reduce_fusion.1
  233.3 5.2 %all_to_all.36 = bf16[2,128,128]{2,1,0:T(8,128)(2,1)S(1)} all-to-all(bf16[2,128,128]{2,1,0:T(8,128)(2,1)S(1)} %pad_maximum_fusion), channel_id=1, replica_groups=mesh['sp_0'=8,'sp_1'=8,'sp_2'=2,'tp'=4] {'sp_2'}, dimensions={0} | all-to-all | bytes 131072 | tf_op jit(solution)/shard_map/all_to_all | solution.py:20
  238.5 0.3 multiply_reduce_fusion.2
  238.8 0.1 multiply_convert_fusion
  238.9 0.1 copy.98
  239.0 1.6 fusion.2
  240.6 11.6 %all_to_all.37 = bf16[4,32,2048]{2,1,0:T(8,128)(2,1)S(1)} all-to-all(bf16[4,32,2048]{2,1,0:T(8,128)(2,1)S(1)} %bitcast.95), channel_id=1, replica_groups=mesh['sp_0'=8,'sp_1'=8,'sp_2'=2,'tp'=4] {'tp'}, dimensions={0} | all-to-all | bytes 1048576 | tf_op jit(solution)/shard_map/all_to_all | solution.py:20
  252.2 0.7 reduce_sum.145
  (59 shorter events, 0.5 us)
Async XLA Ops:
  0.0 221.4 %copy-start = (bf16[256,2048]{1,0:T(8,128)(2,1)S(1)}, bf16[256,2048]{1,0:T(8,128)(2,1)}, u32[]{:S(2)}) copy-start(bf16[256,2048]{1,0:T(8,128)(2,1)} %param.29) | copy-start | bytes 3145732
  1.8 11.8 %all-to-all-start = ((bf16[4,32,2048]{2,1,0:T(8,128)(2,1)}), bf16[4,32,2048]{2,1,0:T(8,128)(2,1)S(1)}, u32[]{:S(2)}, u32[]{:S(2)}) async-start(bf16[4,32,2048]{2,1,0:T(8,128)(2,1)} %broadcast_in_dim.101), calls=%async_computation | async-start | bytes 1048576 | tf_op jit(solution)/shard_map/all_to_all | solution.py:20
  36.5 14.6 %copy-start.1 = (f32[128,256]{1,0:T(8,128)S(1)}, f32[128,256]{1,0:T(8,128)}, u32[]{:S(2)}) copy-start(f32[128,256]{1,0:T(8,128)} %param.26) | copy-start | bytes 393220
  36.5 16.8 %copy-start.4 = (f32[2048]{0:T(1024)S(1)}, f32[2048]{0:T(1024)}, u32[]{:S(2)}) copy-start(f32[2048]{0:T(1024)} %param.17) | copy-start | bytes 24580
  36.5 16.8 %copy-start.3 = (f32[2,128,128]{2,1,0:T(8,128)S(1)}, f32[2,128,128]{2,1,0:T(8,128)}, u32[]{:S(2)}) copy-start(f32[2,128,128]{2,1,0:T(8,128)} %param.28) | copy-start | bytes 393220
  36.5 16.9 %copy-start.6 = (f32[256]{0:T(256)S(1)}, f32[256]{0:T(256)}, u32[]{:S(2)}) copy-start(f32[256]{0:T(256)} %param.25) | copy-start | bytes 3076
  36.5 152.9 %all-to-all-start.2 = ((bf16[16,128,1536]{2,1,0:T(8,128)(2,1)}), bf16[16,128,1536]{2,1,0:T(8,128)(2,1)}, u32[]{:S(2)}, u32[]{:S(2)}) async-start(bf16[16,128,1536]{2,1,0:T(8,128)(2,1)} %stack.25), calls=%async_computation.2 | async-start | bytes 12582912 | tf_op jit(solution)/shard_map/all_to_all | solution.py:107
  51.0 3.2 %copy-start.2 = (bf16[256,256,1]{1,0,2:T(8,128)(2,1)S(1)}, bf16[256,256,1]{1,0,2:T(8,128)(2,1)}, u32[]{:S(2)}) copy-start(bf16[256,256,1]{1,0,2:T(8,128)(2,1)} %constant.72) | copy-start | bytes 393220
  51.0 6.0 %copy-start.5 = (f32[3,256]{1,0:T(4,128)S(1)}, f32[3,256]{1,0:T(4,128)}, u32[]{:S(2)}) copy-start(f32[3,256]{1,0:T(4,128)} %param.21) | copy-start | bytes 9220
  51.1 145.0 %collective-permute-start.2 = (f32[128,128]{1,0:T(8,128)S(1)}, f32[128,128]{1,0:T(8,128)S(1)}, u32[]{:S(2)}, u32[]{:S(2)}) collective-permute-start(f32[128,128]{1,0:T(8,128)S(1)} %constant_dynamic-slice_fusion.1), channel_id=1, source_target_pairs={{0,4},{4,0},{1,5},{5,1},{2,6},{6,2},{3,7},{7,3},{8,12},{12,8},{9,1... | collective-permute-start | bytes 196616 | tf_op jit(solution)/shard_map/ppermute | solution.py:28
  54.8 6.2 %collective-permute-start.1 = (bf16[128,2048]{0,1:T(8,128)(2,1)S(1)}, bf16[128,2048]{0,1:T(8,128)(2,1)}, u32[]{:S(2)}, u32[]{:S(2)}) collective-permute-start(bf16[128,2048]{0,1:T(8,128)(2,1)S(1)} %bitcast.99), channel_id=1, source_target_pairs={{0,4},{4,0},{1,5},{5,1},{2,6},{6,2},{3,7},{7,3},{8,12},{12,8},{9,1... | collective-permute-start | bytes 1572872 | tf_op jit(solution)/shard_map/ppermute | solution.py:28
  57.1 3.5 %collective-permute-start = (bf16[16,2048]{1,0:T(8,128)(2,1)S(1)}, bf16[16,2048]{1,0:T(8,128)(2,1)S(1)}, u32[]{:S(2)}, u32[]{:S(2)}) collective-permute-start(bf16[16,2048]{1,0:T(8,128)(2,1)S(1)} %bitcast.103), channel_id=1, source_target_pairs={{0,4},{4,8},{8,12},{12,16},{16,20},{20,24},{24,28},{28,32},{32,36}... | collective-permute-start | bytes 196616 | tf_op jit(solution)/shard_map/ppermute | solution.py:33
  197.8 41.0 %copy-start.7 = (f32[128]{0:T(128)S(1)}, f32[128]{0:T(128)}, u32[]{:S(2)}) copy-start(f32[128]{0:T(128)} %param.27) | copy-start | bytes 1540
  197.8 14.7 %all-to-all-start.3 = ((bf16[8,144,128]{2,1,0:T(8,128)(2,1)}), bf16[8,144,128]{2,1,0:T(8,128)(2,1)S(1)}, u32[]{:S(2)}, u32[]{:S(2)}) async-start(bf16[8,144,128]{2,1,0:T(8,128)(2,1)} %broadcast_in_dim.107), calls=%async_computation.3 | async-start | bytes 589824 | tf_op jit(solution)/shard_map/all_to_all | solution.py:20
  213.8 19.0 %all-to-all-start.4 = ((bf16[8,144,128]{2,1,0:T(8,128)(2,1)}), bf16[8,144,128]{2,1,0:T(8,128)(2,1)S(1)}, u32[]{:S(2)}, u32[]{:S(2)}) async-start(bf16[8,144,128]{2,1,0:T(8,128)(2,1)} %broadcast_in_dim.111), calls=%async_computation.4 | async-start | bytes 589824 | tf_op jit(solution)/shard_map/all_to_all | solution.py:20
